TPU v7x, 32 devices: a whole 2x2x4 slice. The times are simulated.
32 devices in a mesh: sp: 8 (over z, core), tp: 4 (over y, x).
Axes of the slice: x: 2, y: 2, z: 4, core: 2. Of those that a mesh axis runs over, the one named last changes fastest.
Arguments:
- query_heads: bfloat16 [2048, 1024], P('sp', 'tp'), may hold values from -6 to 6
- key_heads: bfloat16 [2048, 256], P('sp'), may hold values from -6 to 6
- value_heads: bfloat16 [2048, 256], P('sp'), may hold values from -24 to 24
- q_gain: float32 [64], replicated, may hold values from 0.6 to 4.5
- k_gain: float32 [64], replicated, may hold values from 0.6 to 4.5
- out_weight: bfloat16 [1024, 2048], P('tp'), may hold values from -0.1875 to 0.1875
- residual: bfloat16 [2048, 2048], P('sp', 'tp'), may hold values from -3 to 3
- norm_gain: float32 [2048], P('tp'), may hold values from 0.1 to 1.9
- routes: int32 [2048, 2], P('sp'), may hold values from 0 to 7, all different within a row; in each aligned block of 256 rows (0 to 255, 256 to 511, ...) at most 81 rows name the same one
- route_weights: float32 [2048, 2], P('sp'), may hold values from 0.5 to 1.5
- w_gate: bfloat16 [8, 2048, 4096], P('sp', None, 'tp'), may hold values from -0.125 to 0.125
- w_up: bfloat16 [8, 2048, 4096], P('sp', None, 'tp'), may hold values from -0.125 to 0.125
- w_down: bfloat16 [8, 4096, 2048], P('sp', 'tp'), may hold values from -0.1875 to 0.1875
Outputs:
- layer_out: bfloat16 [2048, 2048], P('sp', 'tp')
Inputs may be any that keep to these rules, and one draw needn't show every extreme that they name: `routes`: each row names 2 different experts. Among the 256 rows of one index of sp, no expert is named more than 81 times, a bound that some block reaches.
All inputs are finite; a program needn't handle non-finite values.
Results may differ from a plain program's by a relative error of at most 0.02.
The roundings to bfloat16 on the way count: a program that leaves them out, or rounds other values in their place, can miss the bound.
Values may be sent and summed in bfloat16 or wider, within the bound.
No kernel may reach another device: no remote copies, remote signals or barrier semaphores. Data moves between devices by JAX's collectives and lax.ppermute only.
A program may use at most 64 MiB of HBM per device.

v0:
```python
import jax
import jax.numpy as jnp
from jax import lax
from jax.sharding import PartitionSpec as P

D = 2048
HQ = 16
KV = 4
E = 64
TOPK = 2
GRID_W = 64
norm_eps = 1e-06
rope_base = 10000.0


def normalize(values_f, gain):
    mean_sq = jnp.mean(values_f * values_f, axis=-1, keepdims=True)
    return values_f * lax.rsqrt(mean_sq + norm_eps) * gain


def rotate(values_f, positions):
    head_width = values_f.shape[-1]
    half_width = head_width // 2
    quarter_width = half_width // 2
    frequency = rope_base ** (-jnp.arange(quarter_width, dtype=jnp.float32) / quarter_width)
    grid_rows = (positions // GRID_W).astype(jnp.float32)
    grid_cols = (positions % GRID_W).astype(jnp.float32)
    shape = (values_f.shape[0],) + (1,) * (values_f.ndim - 2) + (quarter_width,)
    pieces = []
    for coords, offset_lo in ((grid_rows, 0), (grid_cols, half_width)):
        angles = coords[:, None] * frequency[None, :]
        cosine = jnp.cos(angles).reshape(shape)
        sines = jnp.sin(angles).reshape(shape)
        first_part = values_f[..., offset_lo : offset_lo + quarter_width]
        second_part = values_f[..., offset_lo + quarter_width : offset_lo + half_width]
        pieces.append(first_part * cosine - second_part * sines)
        pieces.append(second_part * cosine + first_part * sines)
    return jnp.concatenate(pieces, axis=-1)


def shards(
    query_heads,
    key_heads,
    value_heads,
    q_gain,
    k_gain,
    out_weight,
    residual,
    norm_gain,
    routes,
    route_weights,
    w_gate,
    w_up,
    w_down,
):
    tok_rows = query_heads.shape[0]
    head_local = query_heads.shape[1] // E
    group_size = HQ // KV
    kv_count = max(head_local // group_size, 1)
    per_kv = head_local // kv_count
    tp_index = lax.axis_index("tp")
    sp_index = lax.axis_index("sp")
    kv_first = tp_index * head_local // group_size
    positions = sp_index * tok_rows + jnp.arange(tok_rows, dtype=jnp.int32)
    query_f = query_heads.astype(jnp.float32).reshape(tok_rows, kv_count, per_kv, E)
    q_turned = rotate(normalize(query_f, q_gain), positions).astype(jnp.bfloat16)
    key_cols = lax.dynamic_slice_in_dim(key_heads, kv_first * E, kv_count * E, 1)
    value_cols = lax.dynamic_slice_in_dim(value_heads, kv_first * E, kv_count * E, 1)
    key_f = key_cols.astype(jnp.float32).reshape(tok_rows, kv_count, E)
    k_turned = rotate(normalize(key_f, k_gain), positions).astype(jnp.bfloat16)
    value_sel = value_cols.reshape(tok_rows, kv_count, E)
    run_max = jnp.full((kv_count, per_kv, tok_rows), -1e30, jnp.float32)
    key_block = lax.all_gather(k_turned, "sp", axis=0, tiled=True)
    value_block = lax.all_gather(value_sel, "sp", axis=0, tiled=True)
    scores = jnp.einsum(
        "qcge,kce->cgqk", q_turned, key_block, preferred_element_type=jnp.float32
    ) * E ** (-0.5)
    new_max = jnp.maximum(run_max, jnp.max(scores, axis=-1))
    exped = jnp.exp(scores - new_max[..., None])
    denominator = jnp.sum(exped, axis=-1)
    weighted = jnp.einsum(
        "cgqk,kce->cgqe",
        exped.astype(jnp.bfloat16),
        value_block,
        preferred_element_type=jnp.float32,
    )
    run_max, denominator, weighted = (new_max, denominator, weighted)
    attended = (weighted / denominator[..., None]).astype(jnp.bfloat16)
    attended = attended.transpose(2, 0, 1, 3).reshape(tok_rows, head_local * E)
    partial_value = jnp.dot(attended, out_weight, preferred_element_type=jnp.float32).astype(
        jnp.bfloat16
    )
    attn_out = lax.psum_scatter(partial_value, "tp", scatter_dimension=1, tiled=True).astype(
        jnp.float32
    )
    after_attn = residual.astype(jnp.float32) + attn_out
    square_sum = lax.psum(jnp.sum(after_attn * after_attn, axis=1), "tp")
    normed = (after_attn * lax.rsqrt(square_sum / D + norm_eps)[:, None] * norm_gain).astype(
        jnp.bfloat16
    )
    experts_n = lax.axis_size("sp")
    capacity = 5 * tok_rows * TOPK // (4 * experts_n) + 1
    assign = routes.reshape(tok_rows * TOPK)
    onehot = (assign[:, None] == jnp.arange(experts_n, dtype=jnp.int32)[None, :]).astype(jnp.int32)
    before = jnp.cumsum(onehot, axis=0) - onehot
    slot_rank = jnp.sum(before * onehot, axis=1)
    slot_index = assign * capacity + slot_rank
    token_local = jnp.arange(tok_rows * TOPK, dtype=jnp.int32) // TOPK
    slot_token = (
        jnp.full((experts_n * capacity,), tok_rows, jnp.int32).at[slot_index].set(token_local)
    )
    gate_w = w_gate[0]
    up_w = w_up[0]
    down_w = w_down[0]
    padded = jnp.concatenate([normed, jnp.zeros((1, normed.shape[1]), jnp.bfloat16)], axis=0)
    slot_rows = padded[slot_token].reshape(experts_n, capacity, normed.shape[1])
    block_rows = lax.all_gather(
        lax.all_to_all(slot_rows, "sp", split_axis=0, concat_axis=0, tiled=True),
        "tp",
        axis=2,
        tiled=True,
    )
    gate_next = jnp.einsum("scd,df->scf", block_rows, gate_w, preferred_element_type=jnp.float32)
    up_next = jnp.einsum("scd,df->scf", block_rows, up_w, preferred_element_type=jnp.float32)
    activated = (jax.nn.silu(gate_next) * up_next).astype(jnp.bfloat16)
    partials = jnp.einsum(
        "scf,fd->scd", activated, down_w, preferred_element_type=jnp.float32
    ).astype(jnp.bfloat16)
    expert_rows = (
        lax.psum_scatter(partials, "tp", scatter_dimension=2, tiled=True)
        .astype(jnp.float32)
        .astype(jnp.bfloat16)
    )
    returned_rows = lax.all_to_all(expert_rows, "sp", split_axis=0, concat_axis=0, tiled=True)
    columns = returned_rows.shape[2]
    picked = returned_rows.reshape(experts_n * capacity, columns)[slot_index].astype(jnp.float32)
    picked = picked.reshape(tok_rows, TOPK, columns)
    expert_mix = jnp.sum(picked * route_weights[:, :, None], axis=1)
    return (after_attn + expert_mix).astype(jnp.bfloat16)


def solution(mesh):
    return jax.shard_map(
        shards,
        mesh=mesh,
        in_specs=(
            P("sp", "tp"),
            P("sp", None),
            P("sp", None),
            P(),
            P(),
            P("tp", None),
            P("sp", "tp"),
            P("tp"),
            P("sp", None),
            P("sp", None),
            P("sp", None, "tp"),
            P("sp", None, "tp"),
            P("sp", "tp", None),
        ),
        out_specs=P("sp", "tp"),
        check_vma=False,
    )
```

profile of v0, /device:TPU:0, one launch (start us, length us, event | category | flops | bytes accessed | tf_op | source)
XLA Modules:
  0.0 260.0 jit_solution(18293213865418719815)
XLA Ops:
  6.6 1.0 constant_dynamic-slice_fusion.1
  8.9 15.9 %all_gather.9 = bf16[2048,1,64]{0,2,1:T(8,128)(2,1)S(1)} all-gather(bf16[256,1,64]{0,2,1:T(8,128)(2,1)S(1)} %pad_maximum_fusion), channel_id=1, replica_groups=mesh['sp'=8,'tp'=4] {'sp'}, dimensions={0}, use_global_device_ids=true | all-gather | bytes 294912 | tf_op jit(solution)/shard_map/all_gather | solution.py:73
  24.8 1.0 copy.20
  26.7 4.5 %bitcast_reduce_fusion = (f32[4,256]{1,0:T(4,128)S(1)}, f32[2048,256,4]{1,0,2:T(8,128)}) fusion(bf16[256,4,16]{0,2,1:T(8,128)(2,1)S(1)} %get-tuple-element.9, bf16[256,4,16]{0,2,1:T(8,128)(2,1)S(1)} %get-tuple-element.10, bf16[256,4,16]{0,2,1:T(8,128)(2,1)S(1)} %get-tuple-element.6, bf16[256,4,16]{0,2,1:T(8,128)(2,1)S(1)} %get-tuple-element.5, ...), kind=kOutput, calls=%fused_computation.4 | convolution fusion | flops 273153024 | bytes 8785920 | tf_op jit(solution)/shard_map/qcge,kce->cgqk/dot_general | solution.py:75
  31.4 14.2 %all-gather = bf16[2048,64]{0,1:T(8,128)(2,1)S(1)} all-gather(bf16[256,64]{0,1:T(8,128)(2,1)S(1)} %copy.28), channel_id=2, replica_groups=mesh['sp'=8,'tp'=4] {'sp'}, dimensions={0}, use_global_device_ids=true | all-gather | bytes 294912 | tf_op jit(solution)/shard_map/all_gather | solution.py:74
  45.6 4.9 %fusion.1 = f32[4,256]{1,0:T(4,128)S(1)} fusion(f32[2048,256,4]{1,0,2:T(8,128)} %get-tuple-element.24, f32[4,256]{1,0:T(4,128)S(1)} %broadcast_maximum_fusion), kind=kLoop, calls=%fused_computation.6 | loop fusion | flops 6290432 | bytes 8396800 | tf_op jit(solution)/shard_map/reduce_sum | solution.py:80
  51.4 1.5 fusion.20
  52.9 1.5 convolution_convert_fusion
  54.9 1.1 reduce-window.6
  56.7 2.4 scatter_custom_fusion
  59.2 24.4 %reduce-scatter.3.cloned.1.call-done = bf16[256,512]{1,0:T(8,128)(2,1)} async-done(((bf16[256,2048]{1,0:T(8,128)(2,1)}), bf16[256,512]{1,0:T(8,128)(2,1)}) %reduce-scatter.3.cloned.1.call-update) | async-done | bytes 262160 | tf_op jit(solution)/shard_map/reduce_scatter | solution.py:93
  83.6 1.1 multiply_reduce_fusion.1
  84.7 8.9 %psum.7 = f32[256]{0:T(256)S(1)} all-reduce(f32[256]{0:T(256)S(1)} %multiply_reduce_fusion.1), channel_id=1, replica_groups=mesh['sp'=8,'tp'=4] {'tp'}, use_global_device_ids=true, to_apply=%region_6.7 | all-reduce | flops 256 | bytes 2048 | tf_op jit(solution)/shard_map/psum | solution.py:97
  93.7 1.1 multiply_convert_fusion.1
  94.8 2.8 %gather_fusion = bf16[648,512]{1,0:T(8,128)(2,1)S(1)} fusion(bf16[257,512]{1,0:T(8,128)(2,1)S(1)} %concatenate.36, s32[1024]{0:T(1024)S(1)} %pad_clamp_fusion.1), kind=kCustom, calls=%fused_computation | custom fusion | bytes 1329696 | tf_op jit(solution)/shard_map/gather | solution.py:116
  97.8 24.0 %all_to_all.10 = bf16[8,81,512]{2,1,0:T(8,128)(2,1)} all-to-all(bf16[8,81,512]{2,1,0:T(8,128)(2,1)S(1)} %reshape.562), channel_id=1, replica_groups=mesh['sp'=8,'tp'=4] {'sp'}, dimensions={0} | all-to-all | bytes 1327104 | tf_op jit(solution)/shard_map/all_to_all | solution.py:118
  122.1 39.4 %all-gather.3.cloned.1.call-done = bf16[8,81,2048]{2,1,0:T(8,128)(2,1)} async-done(((bf16[8,81,512]{2,1,0:T(8,128)(2,1)}), bf16[8,81,2048]{2,1,0:T(8,128)(2,1)}) %all-gather.3.cloned.1.call-update) | async-done | bytes 2654224 | tf_op jit(solution)/shard_map/all_gather | solution.py:117
  161.5 7.8 %fusion.6 = f32[8,81,1024]{2,1,0:T(8,128)} fusion(bf16[8,81,2048]{2,1,0:T(8,128)(2,1)} %all-gather.3.cloned.1.call-done, bf16[1,2048,1024]{2,1,0:T(8,128)(2,1)} %param.24), kind=kOutput, calls=%fused_computation.11 | convolution fusion | flops 2717908992 | bytes 9502720 | tf_op jit(solution)/shard_map/scd,df->scf/dot_general | solution.py:124
  169.3 13.1 %fusion.12 = bf16[8,81,2048]{2,1,0:T(8,128)(2,1)} fusion(bf16[1,1024,2048]{2,1,0:T(8,128)(2,1)} %param.25, f32[8,81,1024]{2,1,0:T(8,128)} %fusion.6, bf16[8,81,2048]{2,1,0:T(8,128)(2,1)} %all-gather.3.cloned.1.call-done, bf16[1,2048,1024]{2,1,0:T(8,128)(2,1)} %param.23), kind=kOutput, calls=%fused_computation.16 | convolution fusion | flops 5441126400 | bytes 16351232 | tf_op jit(solution)/shard_map/scf,fd->scd/dot_general | solution.py:126
  182.4 41.9 %reduce-scatter.5.cloned.1.call-done = bf16[8,81,512]{2,1,0:T(8,128)(2,1)} async-done(((bf16[8,81,2048]{2,1,0:T(8,128)(2,1)}), bf16[8,81,512]{2,1,0:T(8,128)(2,1)}) %reduce-scatter.5.cloned.1.call-update) | async-done | bytes 663568 | tf_op jit(solution)/shard_map/reduce_scatter | solution.py:130
  224.3 4.6 %all-to-all-start.1 = ((bf16[8,81,512]{2,1,0:T(8,128)(2,1)}), bf16[8,81,512]{2,1,0:T(8,128)(2,1)S(1)}, u32[]{:S(2)}, u32[]{:S(2)}) async-start(bf16[8,81,512]{2,1,0:T(8,128)(2,1)} %reduce-scatter.5.cloned.1.call-done), calls=%async_computation.3 | async-start | bytes 1441792 | tf_op jit(solution)/shard_map/all_to_all | solution.py:134
  229.0 19.4 %all-to-all-done.1 = bf16[8,81,512]{2,1,0:T(8,128)(2,1)S(1)} async-done(((bf16[8,81,512]{2,1,0:T(8,128)(2,1)}), bf16[8,81,512]{2,1,0:T(8,128)(2,1)S(1)}, u32[]{:S(2)}, u32[]{:S(2)}) %all-to-all-start.1) | async-done | bytes 663584 | tf_op jit(solution)/shard_map/all_to_all | solution.py:134
  248.6 2.0 gather_fusion.1
  251.3 1.3 multiply_reduce_fusion
  (61 shorter events, 6.6 us)
Async XLA Ops:
  6.5 46.4 %copy-start = (bf16[256,2048]{1,0:T(8,128)(2,1)S(1)}, bf16[256,2048]{1,0:T(8,128)(2,1)}, u32[]{:S(2)}) copy-start(bf16[256,2048]{1,0:T(8,128)(2,1)} %param.18) | copy-start | bytes 3145732
  6.5 77.1 %reduce-scatter.3.cloned.1.call-start = ((), (), s32[]{:S(2)}) async-start(), calls=%async_computation.4 | async-start | bytes 1310720 | tf_op jit(solution)/shard_map/reduce_scatter | solution.py:93
  26.7 4.5 %copy-start.4 = (bf16[256,256]{1,0:T(8,128)(2,1)S(1)}, bf16[256,256]{1,0:T(8,128)(2,1)}, u32[]{:S(2)}) copy-start(bf16[256,256]{1,0:T(8,128)(2,1)} %param.15) | copy-start | bytes 393220
  45.6 5.8 %copy-start.1 = (f32[2048,256,4]{1,0,2:T(8,128)S(1)}, f32[2048,256,4]{1,0,2:T(8,128)}, u32[]{:S(2)}) copy-start(f32[2048,256,4]{1,0,2:T(8,128)} %get-tuple-element.24) | copy-start | bytes 25165828
  51.4 3.1 %copy-start.5 = (s32[256,2]{0,1:T(2,128)S(1)}, s32[256,2]{0,1:T(2,128)}, u32[]{:S(2)}) copy-start(s32[256,2]{0,1:T(2,128)} %param.21) | copy-start | bytes 6148
  52.9 30.7 %copy-start.2 = (bf16[256,512]{1,0:T(8,128)(2,1)S(1)}, bf16[256,512]{1,0:T(8,128)(2,1)}, u32[]{:S(2)}) copy-start(bf16[256,512]{1,0:T(8,128)(2,1)} %param.19) | copy-start | bytes 786436
  52.9 40.8 %copy-start.6 = (f32[512]{0:T(512)S(1)}, f32[512]{0:T(512)}, u32[]{:S(2)}) copy-start(f32[512]{0:T(512)} %param.20) | copy-start | bytes 6148
  54.4 107.1 %all-gather.3.cloned.1.call-start = ((), (), s32[]{:S(2)}) async-start(), calls=%async_computation.5 | async-start | bytes 3604480 | tf_op jit(solution)/shard_map/all_gather | solution.py:117
  121.9 102.4 %reduce-scatter.5.cloned.1.call-start = ((), (), s32[]{:S(2)}) async-start(), calls=%async_computation.6 | async-start | bytes 3604480 | tf_op jit(solution)/shard_map/reduce_scatter | solution.py:130
  182.4 46.5 %copy-start.7 = (f32[256,2]{0,1:T(2,128)S(1)}, f32[256,2]{0,1:T(2,128)}, u32[]{:S(2)}) copy-start(f32[256,2]{0,1:T(2,128)} %param.22) | copy-start | bytes 6148
  224.3 24.1 %all-to-all-start.1 = ((bf16[8,81,512]{2,1,0:T(8,128)(2,1)}), bf16[8,81,512]{2,1,0:T(8,128)(2,1)S(1)}, u32[]{:S(2)}, u32[]{:S(2)}) async-start(bf16[8,81,512]{2,1,0:T(8,128)(2,1)} %reduce-scatter.5.cloned.1.call-done), calls=%async_computation.3 | async-start | bytes 1441792 | tf_op jit(solution)/shard_map/all_to_all | solution.py:134
  248.6 4.0 %copy-start.3 = (bf16[256,512]{1,0:T(8,128)(2,1)S(1)}, bf16[256,512]{1,0:T(8,128)(2,1)}, u32[]{:S(2)}) copy-start(bf16[256,512]{1,0:T(8,128)(2,1)} %reduce-scatter.3.cloned.1.call-done) | copy-start | bytes 786436
Sparse Core Ops, SparseCore 0:
  54.5 29.0 reduce-scatter.2
  122.0 39.4 all-gather.2
  182.5 41.6 reduce-scatter.4
where the time goes:
time: 260 us
  waiting for transfers between devices  125 us (48%)
  blocking collectives  63.1 us (24%)
  matrix products  28.3 us (11%)
  between operations  13.4 us (5%)
  other arithmetic  12.6 us (5%)
  local copies, waits for them, and re-layouts  12.5 us (5%)
  starting transfers between devices  4.87 us (2%)
    reduce_scatter x1, waiting for transfers between devices, shards(): lax.psum_scatter(partials, 'tp', scatter_dimension=2, tiled=True)  41.9 us
    all_gather x1, waiting for transfers between devices, shards(): lax.all_gather(lax.all_to_all(slot_rows, 'sp', split_axis=0, concat_axis=...  39.4 us
    reduce_scatter x1, waiting for transfers between devices, shards(): lax.psum_scatter(partial_value, 'tp', scatter_dimension=1, tiled=True)  24.4 us
    all_to_all x1, blocking collectives, shards(): lax.all_to_all(slot_rows, 'sp', split_axis=0, concat_axis=0, tiled=True)  24 us
    all_to_all x1, waiting for transfers between devices, shards(): lax.all_to_all(expert_rows, 'sp', split_axis=0, concat_axis=0, tiled=True)  19.4 us
    all_gather x1, blocking collectives, shards(): key_block = lax.all_gather(k_turned, 'sp', axis=0, tiled=True)  15.9 us
    all_gather x1, blocking collectives, shards(): value_block = lax.all_gather(value_sel, 'sp', axis=0, tiled=True)  14.2 us
    dot_general x1, matrix products, shards(): jnp.einsum('scf,fd->scd', activated, down_w, preferred_element_type=jnp.f...  13.1 us
  transfers between devices with their start and end apart: 4, of which 4 were waited for; matrix products, arithmetic and copies ran while one was open for 2% of the time, Pallas kernels for 0%

commit v1 on v0

--- a/solution.py
+++ b/solution.py
@@ -11,6 +11,16 @@
 GRID_W = 64
 norm_eps = 1e-06
 rope_base = 10000.0
+
+
+def around_the_ring(x, mesh_axis, dim):
+    size = lax.axis_size(mesh_axis)
+    held, blocks = (x, [x])
+    for _ in range(size - 1):
+        held = lax.ppermute(held, mesh_axis, [(i, (i + 1) % size) for i in range(size)])
+        blocks.insert(0, held)
+    line = jnp.concatenate(blocks, axis=dim)
+    return jnp.roll(line, (lax.axis_index(mesh_axis) + 1) * x.shape[dim], axis=dim)
 
 
 def normalize(values_f, gain):
@@ -71,7 +81,7 @@
     value_sel = value_cols.reshape(tok_rows, kv_count, E)
     run_max = jnp.full((kv_count, per_kv, tok_rows), -1e30, jnp.float32)
     key_block = lax.all_gather(k_turned, "sp", axis=0, tiled=True)
-    value_block = lax.all_gather(value_sel, "sp", axis=0, tiled=True)
+    value_block = around_the_ring(value_sel, "sp", 0)
     scores = jnp.einsum(
         "qcge,kce->cgqk", q_turned, key_block, preferred_element_type=jnp.float32
     ) * E ** (-0.5)

time: 260 us -> 264 us (1.015)
  waiting for transfers between devices: 125 us -> 148 us
  blocking collectives: 63.1 us -> 47.3 us
  other arithmetic: 12.6 us -> 9.04 us
    ppermute x0 -> x7, waiting for transfers between devices: none -> 25 us  [around_the_ring(): lax.ppermute(held, mesh_axis, [(i, (i + 1) % size) for i in range(size)])]
    all_gather x1 -> x0, blocking collectives: 14.2 us -> none  [shards(): value_block = lax.all_gather(value_sel, 'sp', axis=0, tiled=True)]
    reduce_sum x1, other arithmetic: 4.9 us -> 1.39 us  [shards(): denominator = jnp.sum(exped, axis=-1)]
    dot_general x1, matrix products: 1.52 us -> 4.9 us  [shards(): jnp.einsum('cgqk,kce->cgqe', exped.astype(jnp.bfloat16), value_block, pre...]
    dot_general x1, matrix products: 4.51 us -> 1.29 us  [shards(): jnp.einsum('qcge,kce->cgqk', q_turned, key_block, preferred_element_type=...]
  transfers between devices with their start and end apart: 4 -> 11, of which waited for: 4 -> 10; matrix products, arithmetic and copies ran while one was open for 2% -> 4% of each run, Pallas kernels for 0% -> 0%
where the time goes in v1:
time: 264 us
  waiting for transfers between devices  148 us (56%)
  blocking collectives  47.3 us (18%)
  matrix products  28.5 us (11%)
  between operations  13.5 us (5%)
  local copies, waits for them, and re-layouts  11.7 us (4%)
  other arithmetic  9.04 us (3%)
  starting transfers between devices  5.84 us (2%)
    reduce_scatter x1, waiting for transfers between devices, shards(): lax.psum_scatter(partials, 'tp', scatter_dimension=2, tiled=True)  41.9 us
    all_gather x1, waiting for transfers between devices, shards(): lax.all_gather(lax.all_to_all(slot_rows, 'sp', split_axis=0, concat_axis=...  39.4 us
    ppermute x7, waiting for transfers between devices, around_the_ring(): lax.ppermute(held, mesh_axis, [(i, (i + 1) % size) for i in range(size)])  25 us
    all_to_all x1, blocking collectives, shards(): lax.all_to_all(slot_rows, 'sp', split_axis=0, concat_axis=0, tiled=True)  24 us
    reduce_scatter x1, waiting for transfers between devices, shards(): lax.psum_scatter(partial_value, 'tp', scatter_dimension=1, tiled=True)  22 us
    all_to_all x1, waiting for transfers between devices, shards(): lax.all_to_all(expert_rows, 'sp', split_axis=0, concat_axis=0, tiled=True)  19.4 us
    all_gather x1, blocking collectives, shards(): key_block = lax.all_gather(k_turned, 'sp', axis=0, tiled=True)  14.3 us
    dot_general x1, matrix products, shards(): jnp.einsum('scf,fd->scd', activated, down_w, preferred_element_type=jnp.f...  13.1 us
  transfers between devices with their start and end apart: 11, of which 10 were waited for; matrix products, arithmetic and copies ran while one was open for 4% of the time, Pallas kernels for 0%

profile of v1, /device:TPU:0, one launch (start us, length us, event | category | flops | bytes accessed | tf_op | source)
XLA Modules:
  0.0 263.6 jit_solution(11071637668057635384)
XLA Ops:
  11.2 2.7 %collective-permute-done = bf16[256,1,64]{0,2,1:T(8,128)(2,1)S(1)} collective-permute-done((bf16[256,1,64]{0,2,1:T(8,128)(2,1)S(1)}, bf16[256,1,64]{0,2,1:T(8,128)(2,1)S(1)}, u32[]{:S(2)}, u32[]{:S(2)}) %collective-permute-start) | collective-permute-done | bytes 32800 | tf_op jit(solution)/shard_map/ppermute | solution.py:20
  14.1 4.9 %collective-permute-done.1 = bf16[256,1,64]{0,2,1:T(8,128)(2,1)S(1)} collective-permute-done((bf16[256,1,64]{0,2,1:T(8,128)(2,1)S(1)}, bf16[256,1,64]{0,2,1:T(8,128)(2,1)S(1)}, u32[]{:S(2)}, u32[]{:S(2)}) %collective-permute-start.1) | collective-permute-done | bytes 32800 | tf_op jit(solution)/shard_map/ppermute | solution.py:20
  19.0 5.1 %collective-permute-done.2 = bf16[256,1,64]{0,2,1:T(8,128)(2,1)S(1)} collective-permute-done((bf16[256,1,64]{0,2,1:T(8,128)(2,1)S(1)}, bf16[256,1,64]{0,2,1:T(8,128)(2,1)S(1)}, u32[]{:S(2)}, u32[]{:S(2)}) %collective-permute-start.2) | collective-permute-done | bytes 32800 | tf_op jit(solution)/shard_map/ppermute | solution.py:20
  24.2 14.3 %all_gather.6 = bf16[2048,1,64]{0,2,1:T(8,128)(2,1)S(1)} all-gather(bf16[256,1,64]{0,2,1:T(8,128)(2,1)S(1)} %pad_maximum_fusion), channel_id=1, replica_groups=mesh['sp'=8,'tp'=4] {'sp'}, dimensions={0}, use_global_device_ids=true | all-gather | bytes 294912 | tf_op jit(solution)/shard_map/all_gather | solution.py:83
  38.8 1.3 bitcast_reduce_fusion
  40.1 3.5 %collective-permute-done.4 = bf16[256,1,64]{0,2,1:T(8,128)(2,1)S(1)} collective-permute-done((bf16[256,1,64]{0,2,1:T(8,128)(2,1)S(1)}, bf16[256,1,64]{0,2,1:T(8,128)(2,1)S(1)}, u32[]{:S(2)}, u32[]{:S(2)}) %collective-permute-start.4) | collective-permute-done | bytes 32800 | tf_op jit(solution)/shard_map/ppermute | solution.py:20
  43.6 5.1 %collective-permute-done.5 = bf16[256,1,64]{0,2,1:T(8,128)(2,1)S(1)} collective-permute-done((bf16[256,1,64]{0,2,1:T(8,128)(2,1)S(1)}, bf16[256,1,64]{0,2,1:T(8,128)(2,1)S(1)}, u32[]{:S(2)}, u32[]{:S(2)}) %collective-permute-start.5) | collective-permute-done | bytes 32800 | tf_op jit(solution)/shard_map/ppermute | solution.py:20
  48.7 1.4 fusion.1
  50.1 3.7 %collective-permute-done.6 = bf16[256,1,64]{0,2,1:T(8,128)(2,1)S(1)} collective-permute-done((bf16[256,1,64]{0,2,1:T(8,128)(2,1)S(1)}, bf16[256,1,64]{0,2,1:T(8,128)(2,1)S(1)}, u32[]{:S(2)}, u32[]{:S(2)}) %collective-permute-start.6) | collective-permute-done | bytes 32800 | tf_op jit(solution)/shard_map/ppermute | solution.py:20
  54.1 4.9 %fusion.20 = bf16[4,256,64]{1,2,0:T(8,128)(2,1)S(1)} fusion(f32[2048,256,4]{1,0,2:T(8,128)} %copy-done.1, f32[4,256]{1,0:T(4,128)S(1)} %broadcast_maximum_fusion, bf16[4096,1,64]{0,2,1:T(8,128)(2,1)S(1)} %constant_dynamic-update-slice_fusion, s32[]{:T(128)S(6)} %select_n.67, f32[4,256]{1,0:T(4,128)S(1)} %fusion.1), kind=kOutput, calls=%fused_computation.20 | convolution fusion | flops 274857984 | bytes 8790020 | tf_op jit(solution)/shard_map/cgqk,kce->cgqe/dot_general | solution.py:91
  59.0 1.5 convolution_convert_fusion
  62.8 2.4 scatter_custom_fusion
  65.3 22.0 %reduce-scatter.3.cloned.1.call-done = bf16[256,512]{1,0:T(8,128)(2,1)} async-done(((bf16[256,2048]{1,0:T(8,128)(2,1)}), bf16[256,512]{1,0:T(8,128)(2,1)}) %reduce-scatter.3.cloned.1.call-update) | async-done | bytes 262160 | tf_op jit(solution)/shard_map/reduce_scatter | solution.py:103
  88.4 8.9 %psum.7 = f32[256]{0:T(256)S(1)} all-reduce(f32[256]{0:T(256)S(1)} %multiply_reduce_fusion.1), channel_id=1, replica_groups=mesh['sp'=8,'tp'=4] {'tp'}, use_global_device_ids=true, to_apply=%region_6.7 | all-reduce | flops 256 | bytes 2048 | tf_op jit(solution)/shard_map/psum | solution.py:107
  98.4 2.8 %gather_fusion = bf16[648,512]{1,0:T(8,128)(2,1)S(1)} fusion(bf16[257,512]{1,0:T(8,128)(2,1)S(1)} %concatenate.43, s32[1024]{0:T(1024)S(1)} %pad_clamp_fusion.1), kind=kCustom, calls=%fused_computation | custom fusion | bytes 1329696 | tf_op jit(solution)/shard_map/gather | solution.py:126
  101.5 24.0 %all_to_all.10 = bf16[8,81,512]{2,1,0:T(8,128)(2,1)} all-to-all(bf16[8,81,512]{2,1,0:T(8,128)(2,1)S(1)} %reshape.562), channel_id=1, replica_groups=mesh['sp'=8,'tp'=4] {'sp'}, dimensions={0} | all-to-all | bytes 1327104 | tf_op jit(solution)/shard_map/all_to_all | solution.py:128
  125.8 39.4 %all-gather.2.cloned.1.call-done = bf16[8,81,2048]{2,1,0:T(8,128)(2,1)} async-done(((bf16[8,81,512]{2,1,0:T(8,128)(2,1)}), bf16[8,81,2048]{2,1,0:T(8,128)(2,1)}) %all-gather.2.cloned.1.call-update) | async-done | bytes 2654224 | tf_op jit(solution)/shard_map/all_gather | solution.py:127
  165.2 7.8 %fusion.6 = f32[8,81,1024]{2,1,0:T(8,128)} fusion(bf16[8,81,2048]{2,1,0:T(8,128)(2,1)} %all-gather.2.cloned.1.call-done, bf16[1,2048,1024]{2,1,0:T(8,128)(2,1)} %param.24), kind=kOutput, calls=%fused_computation.11 | convolution fusion | flops 2717908992 | bytes 9502720 | tf_op jit(solution)/shard_map/scd,df->scf/dot_general | solution.py:134
  173.0 13.1 %fusion.12 = bf16[8,81,2048]{2,1,0:T(8,128)(2,1)} fusion(bf16[1,1024,2048]{2,1,0:T(8,128)(2,1)} %param.25, f32[8,81,1024]{2,1,0:T(8,128)} %fusion.6, bf16[8,81,2048]{2,1,0:T(8,128)(2,1)} %all-gather.2.cloned.1.call-done, bf16[1,2048,1024]{2,1,0:T(8,128)(2,1)} %param.23), kind=kOutput, calls=%fused_computation.16 | convolution fusion | flops 5441126400 | bytes 16351232 | tf_op jit(solution)/shard_map/scf,fd->scd/dot_general | solution.py:136
  186.1 41.9 %reduce-scatter.5.cloned.1.call-done = bf16[8,81,512]{2,1,0:T(8,128)(2,1)} async-done(((bf16[8,81,2048]{2,1,0:T(8,128)(2,1)}), bf16[8,81,512]{2,1,0:T(8,128)(2,1)}) %reduce-scatter.5.cloned.1.call-update) | async-done | bytes 663568 | tf_op jit(solution)/shard_map/reduce_scatter | solution.py:140
  227.9 4.6 %all-to-all-start.1 = ((bf16[8,81,512]{2,1,0:T(8,128)(2,1)}), bf16[8,81,512]{2,1,0:T(8,128)(2,1)S(1)}, u32[]{:S(2)}, u32[]{:S(2)}) async-start(bf16[8,81,512]{2,1,0:T(8,128)(2,1)} %reduce-scatter.5.cloned.1.call-done), calls=%async_computation.3 | async-start | bytes 1441792 | tf_op jit(solution)/shard_map/all_to_all | solution.py:144
  232.7 19.4 %all-to-all-done.1 = bf16[8,81,512]{2,1,0:T(8,128)(2,1)S(1)} async-done(((bf16[8,81,512]{2,1,0:T(8,128)(2,1)}), bf16[8,81,512]{2,1,0:T(8,128)(2,1)S(1)}, u32[]{:S(2)}, u32[]{:S(2)}) %all-to-all-start.1) | async-done | bytes 663584 | tf_op jit(solution)/shard_map/all_to_all | solution.py:144
  252.3 2.0 gather_fusion.1
  255.0 1.3 multiply_reduce_fusion
  (87 shorter events, 12.1 us)
Async XLA Ops:
  6.5 52.4 %copy-start = (bf16[256,2048]{1,0:T(8,128)(2,1)S(1)}, bf16[256,2048]{1,0:T(8,128)(2,1)}, u32[]{:S(2)}) copy-start(bf16[256,2048]{1,0:T(8,128)(2,1)} %param.18) | copy-start | bytes 3145732
  6.5 80.7 %reduce-scatter.3.cloned.1.call-start = ((), (), s32[]{:S(2)}) async-start(), calls=%async_computation.4 | async-start | bytes 1310720 | tf_op jit(solution)/shard_map/reduce_scatter | solution.py:103
  7.7 6.2 %collective-permute-start = (bf16[256,1,64]{0,2,1:T(8,128)(2,1)S(1)}, bf16[256,1,64]{0,2,1:T(8,128)(2,1)S(1)}, u32[]{:S(2)}, u32[]{:S(2)}) collective-permute-start(bf16[256,1,64]{0,2,1:T(8,128)(2,1)S(1)} %bitcast.90), channel_id=1, source_target_pairs={{0,4},{4,8},{8,12},{12,16},{16,20},{20,24},{24,28},{28,0},{1,5},{5... | collective-permute-start | bytes 98312 | tf_op jit(solution)/shard_map/ppermute | solution.py:20
  13.9 5.1 %collective-permute-start.1 = (bf16[256,1,64]{0,2,1:T(8,128)(2,1)S(1)}, bf16[256,1,64]{0,2,1:T(8,128)(2,1)S(1)}, u32[]{:S(2)}, u32[]{:S(2)}) collective-permute-start(bf16[256,1,64]{0,2,1:T(8,128)(2,1)S(1)} %collective-permute-done), channel_id=1, source_target_pairs={{0,4},{4,8},{8,12},{12,16},{16,20},{20,24},{24,28},{28,0},{1,5},{5... | collective-permute-start | bytes 98312 | tf_op jit(solution)/shard_map/ppermute | solution.py:20
  19.0 5.1 %collective-permute-start.2 = (bf16[256,1,64]{0,2,1:T(8,128)(2,1)S(1)}, bf16[256,1,64]{0,2,1:T(8,128)(2,1)S(1)}, u32[]{:S(2)}, u32[]{:S(2)}) collective-permute-start(bf16[256,1,64]{0,2,1:T(8,128)(2,1)S(1)} %collective-permute-done.1), channel_id=1, source_target_pairs={{0,4},{4,8},{8,12},{12,16},{16,20},{20,24},{24,28},{28,0},{1,5},{5... | collective-permute-start | bytes 98312 | tf_op jit(solution)/shard_map/ppermute | solution.py:20
  24.2 14.3 %collective-permute-start.3 = (bf16[256,1,64]{0,2,1:T(8,128)(2,1)S(1)}, bf16[256,1,64]{0,2,1:T(8,128)(2,1)S(1)}, u32[]{:S(2)}, u32[]{:S(2)}) collective-permute-start(bf16[256,1,64]{0,2,1:T(8,128)(2,1)S(1)} %collective-permute-done.2), channel_id=1, source_target_pairs={{0,4},{4,8},{8,12},{12,16},{16,20},{20,24},{24,28},{28,0},{1,5},{5... | collective-permute-start | bytes 98312 | tf_op jit(solution)/shard_map/ppermute | solution.py:20
  38.4 5.1 %collective-permute-start.4 = (bf16[256,1,64]{0,2,1:T(8,128)(2,1)S(1)}, bf16[256,1,64]{0,2,1:T(8,128)(2,1)S(1)}, u32[]{:S(2)}, u32[]{:S(2)}) collective-permute-start(bf16[256,1,64]{0,2,1:T(8,128)(2,1)S(1)} %collective-permute-done.3), channel_id=1, source_target_pairs={{0,4},{4,8},{8,12},{12,16},{16,20},{20,24},{24,28},{28,0},{1,5},{5... | collective-permute-start | bytes 98312 | tf_op jit(solution)/shard_map/ppermute | solution.py:20
  40.1 8.6 %copy-start.1 = (f32[2048,256,4]{1,0,2:T(8,128)}, f32[2048,256,4]{1,0,2:T(8,128)S(1)}, u32[]{:S(2)}) copy-start(f32[2048,256,4]{1,0,2:T(8,128)S(1)} %get-tuple-element.24) | copy-start | bytes 25165828
  43.6 5.1 %collective-permute-start.5 = (bf16[256,1,64]{0,2,1:T(8,128)(2,1)S(1)}, bf16[256,1,64]{0,2,1:T(8,128)(2,1)S(1)}, u32[]{:S(2)}, u32[]{:S(2)}) collective-permute-start(bf16[256,1,64]{0,2,1:T(8,128)(2,1)S(1)} %collective-permute-done.4), channel_id=1, source_target_pairs={{0,4},{4,8},{8,12},{12,16},{16,20},{20,24},{24,28},{28,0},{1,5},{5... | collective-permute-start | bytes 98312 | tf_op jit(solution)/shard_map/ppermute | solution.py:20
  48.7 5.1 %collective-permute-start.6 = (bf16[256,1,64]{0,2,1:T(8,128)(2,1)S(1)}, bf16[256,1,64]{0,2,1:T(8,128)(2,1)S(1)}, u32[]{:S(2)}, u32[]{:S(2)}) collective-permute-start(bf16[256,1,64]{0,2,1:T(8,128)(2,1)S(1)} %collective-permute-done.5), channel_id=1, source_target_pairs={{0,4},{4,8},{8,12},{12,16},{16,20},{20,24},{24,28},{28,0},{1,5},{5... | collective-permute-start | bytes 98312 | tf_op jit(solution)/shard_map/ppermute | solution.py:20
  54.0 6.5 %copy-start.4 = (s32[256,2]{0,1:T(2,128)S(1)}, s32[256,2]{0,1:T(2,128)}, u32[]{:S(2)}) copy-start(s32[256,2]{0,1:T(2,128)} %param.21) | copy-start | bytes 6148
  59.0 28.3 %copy-start.2 = (bf16[256,512]{1,0:T(8,128)(2,1)S(1)}, bf16[256,512]{1,0:T(8,128)(2,1)}, u32[]{:S(2)}) copy-start(bf16[256,512]{1,0:T(8,128)(2,1)} %param.19) | copy-start | bytes 786436
  59.0 38.4 %copy-start.5 = (f32[512]{0:T(512)S(1)}, f32[512]{0:T(512)}, u32[]{:S(2)}) copy-start(f32[512]{0:T(512)} %param.20) | copy-start | bytes 6148
  60.5 104.7 %all-gather.2.cloned.1.call-start = ((), (), s32[]{:S(2)}) async-start(), calls=%async_computation.5 | async-start | bytes 3604480 | tf_op jit(solution)/shard_map/all_gather | solution.py:127
  125.5 102.4 %reduce-scatter.5.cloned.1.call-start = ((), (), s32[]{:S(2)}) async-start(), calls=%async_computation.6 | async-start | bytes 3604480 | tf_op jit(solution)/shard_map/reduce_scatter | solution.py:140
  186.0 46.5 %copy-start.6 = (f32[256,2]{0,1:T(2,128)S(1)}, f32[256,2]{0,1:T(2,128)}, u32[]{:S(2)}) copy-start(f32[256,2]{0,1:T(2,128)} %param.22) | copy-start | bytes 6148
  227.9 24.2 %all-to-all-start.1 = ((bf16[8,81,512]{2,1,0:T(8,128)(2,1)}), bf16[8,81,512]{2,1,0:T(8,128)(2,1)S(1)}, u32[]{:S(2)}, u32[]{:S(2)}) async-start(bf16[8,81,512]{2,1,0:T(8,128)(2,1)} %reduce-scatter.5.cloned.1.call-done), calls=%async_computation.3 | async-start | bytes 1441792 | tf_op jit(solution)/shard_map/all_to_all | solution.py:144
  252.3 4.0 %copy-start.3 = (bf16[256,512]{1,0:T(8,128)(2,1)S(1)}, bf16[256,512]{1,0:T(8,128)(2,1)}, u32[]{:S(2)}) copy-start(bf16[256,512]{1,0:T(8,128)(2,1)} %reduce-scatter.3.cloned.1.call-done) | copy-start | bytes 786436
Sparse Core Ops, SparseCore 0:
  60.6 26.6 reduce-scatter.2
  125.6 39.4 all-gather.1
  186.2 41.7 reduce-scatter.4
